TPU v7x, 512 devices: a 8x2x16 block of a 8x16x16 slice. The times are simulated.
512 devices in a mesh: grp: 2 (over y), sp: 16 (over z), tp: 16 (over x, core).
Axes of the slice: x: 8, y: 2, z: 16, core: 2. Of those that a mesh axis runs over, the one named last changes fastest.
The devices are a block of a 8x16x16 slice.
Arguments:
- target: bfloat16 [4096, 2048], P(('grp', 'sp', 'tp')), parts along dimension 0, may hold values from -6 to 6
- source: bfloat16 [32768, 2048], P(('grp', 'sp', 'tp')), parts along dimension 0, may hold values from -6 to 6
- norm_gain: float32 [2048], replicated, may hold values from 0.1 to 1.9
- query_weight: bfloat16 [2048, 2048], P(None, 'tp'), may hold values from -0.125 to 0.125
- key_weight: bfloat16 [2048, 256], replicated, may hold values from -0.125 to 0.125
- value_weight: bfloat16 [2048, 256], replicated, may hold values from -0.125 to 0.125
- output_weight: bfloat16 [2048, 2048], P('tp'), may hold values from -0.125 to 0.125
- saved_out: bfloat16 [4096, 2048], P(('grp', 'sp'), 'tp'), parts along dimension 0, may hold values from -3 to 3
- log_shift: float32 [16, 4096], P('tp', ('grp', 'sp')), parts along dimension 1, may hold values from 0 to 2
- out_grad: bfloat16 [4096, 2048], P(('grp', 'sp', 'tp')), parts along dimension 0, may hold values from -48 to 48
Outputs:
- target_grad: float32 [4096, 2048], P(('grp', 'sp', 'tp')), parts along dimension 0
- source_grad: float32 [32768, 2048], P(('grp', 'sp', 'tp')), parts along dimension 0
- query_weight_grad: float32 [4096, 2048], P(('grp', 'sp'), 'tp'), parts along dimension 0
There are 2 independent parts, one for each index of `grp`. A program takes and returns all parts, laid end to end along the dimension named above; an argument that names none is the same for every part. Nothing has to cross between parts.
All inputs are finite; a program needn't handle non-finite values.
Results may differ from a plain program's by a relative error of at most 0.02.
Values may be sent and summed in bfloat16 or wider, within the bound.
A program may use at most 64 MiB of HBM per device.

v0:
```python
import jax
import jax.numpy as jnp
from jax import lax
from jax.sharding import PartitionSpec as P

HEADS = 16
HEAD_DIM = 128
KV_HEADS = 2


def cut_along(array, dim, count):
    dims = array.shape
    blocks = array.reshape(*dims[:dim], count, dims[dim] // count, *dims[dim + 1 :])
    return jnp.moveaxis(blocks, dim, 0)


def summed_on_arrival(array, axis, dim):
    blocks = cut_along(array, dim, lax.axis_size(axis))
    arrived = lax.all_to_all(blocks, axis, split_axis=0, concat_axis=0, tiled=True)
    return arrived.astype(jnp.float32).sum(axis=0)


def attend(query_heads, back_heads, shift_cols, drop_cols, key_rows, values, offset):
    factor = HEAD_DIM ** (-0.5)
    scores = (
        jnp.einsum("nhd,md->hnm", query_heads, key_rows, preferred_element_type=jnp.float32)
        * factor
    )
    prob = jnp.exp(scores - shift_cols.T[:, :, None] - offset)
    prob_grad = jnp.einsum("nhd,md->hnm", back_heads, values, preferred_element_type=jnp.float32)
    score_grad = (prob * (prob_grad - drop_cols.T[:, :, None]) * factor).astype(jnp.bfloat16)
    return (prob.astype(jnp.bfloat16), score_grad)


def shards(
    target,
    source,
    norm_gain,
    query_weight,
    key_weight,
    value_weight,
    output_weight,
    saved_out,
    log_shift,
    out_grad,
):
    tp_count = lax.axis_size("tp")
    sp_count = lax.axis_size("sp")
    local_heads = query_weight.shape[1] // HEAD_DIM
    head_width = local_heads * HEAD_DIM
    model_width = target.shape[1]
    group_size = HEADS // KV_HEADS
    pair_index = lax.axis_index("tp") * local_heads // group_size
    offset = jnp.log(jnp.float32(source.shape[0] * tp_count * sp_count))
    target_wide = target.astype(jnp.float32)
    root_mean = jnp.sqrt(jnp.mean(target_wide * target_wide, axis=1, keepdims=True) + 1e-06)
    normed = (target_wide / root_mean * norm_gain).astype(jnp.bfloat16)
    joined = jnp.concatenate([normed, out_grad], axis=1)
    portion = lax.all_gather(joined, "tp", axis=0, tiled=True)
    normed_part = portion[:, :model_width]
    query_part = jnp.dot(normed_part, query_weight, preferred_element_type=jnp.float32).astype(
        jnp.bfloat16
    )
    back_part = lax.dot_general(
        portion[:, model_width:],
        output_weight,
        (((1,), (1,)), ((), ())),
        preferred_element_type=jnp.float32,
    ).astype(jnp.bfloat16)
    gathered = jnp.concatenate([query_part, back_part, normed_part], axis=1)
    queries = gathered[:, :head_width]
    out_back = gathered[:, head_width : 2 * head_width]
    normed_all = gathered[:, 2 * head_width :]
    tgt_local = queries.shape[0]
    key_cols = lax.dynamic_slice_in_dim(key_weight, pair_index * HEAD_DIM, HEAD_DIM, 1)
    value_cols = lax.dynamic_slice_in_dim(value_weight, pair_index * HEAD_DIM, HEAD_DIM, 1)
    both_cols = jnp.concatenate([key_cols, value_cols], axis=1)
    paired = jnp.dot(
        lax.all_gather(source, "tp", axis=0, tiled=True),
        both_cols,
        preferred_element_type=jnp.float32,
    ).astype(jnp.bfloat16)
    key_rows = paired[:, :HEAD_DIM]
    values = paired[:, HEAD_DIM:]
    products = out_back.astype(jnp.float32) * saved_out.astype(jnp.float32)
    drop_cols = jnp.sum(products.reshape(tgt_local, local_heads, HEAD_DIM), axis=2)
    shift_cols = log_shift.T
    portion = (
        lax.all_gather(queries, "sp", axis=0, tiled=True),
        lax.all_gather(out_back, "sp", axis=0, tiled=True),
        lax.all_gather(shift_cols.astype(jnp.bfloat16), "sp", axis=0, tiled=True).astype(
            jnp.float32
        ),
        lax.all_gather(drop_cols.astype(jnp.bfloat16), "sp", axis=0, tiled=True).astype(
            jnp.float32
        ),
    )
    query_part, back_part, shift_part, drop_part = portion
    count_rows = query_part.shape[0]
    query_three = query_part.reshape(count_rows, local_heads, HEAD_DIM)
    back_three = back_part.reshape(count_rows, local_heads, HEAD_DIM)
    prob_low, score_grad = attend(
        query_three, back_three, shift_part, drop_part, key_rows, values, offset
    )
    key_sum = jnp.einsum("hnm,nhd->md", score_grad, query_three, preferred_element_type=jnp.float32)
    value_sum = jnp.einsum("hnm,nhd->md", prob_low, back_three, preferred_element_type=jnp.float32)
    key_sum, value_sum, score_grad = (key_sum, value_sum, score_grad)
    count_rows = portion[0].shape[0]
    added = jnp.einsum(
        "hnm,md->nhd", score_grad, key_rows, preferred_element_type=jnp.float32
    ).reshape(count_rows, head_width)
    query_sum = summed_on_arrival(added.astype(jnp.bfloat16), "sp", 0)
    query_grad = query_sum.astype(jnp.bfloat16)
    stacked = jnp.concatenate([key_sum, value_sum], axis=1)[:, None, :]
    received = lax.all_to_all(
        stacked.astype(jnp.bfloat16), "tp", split_axis=0, concat_axis=1, tiled=True
    ).astype(stacked.dtype)
    own_rows = received.shape[0]
    grouped = jnp.sum(
        received.reshape(own_rows, KV_HEADS, tp_count // KV_HEADS, 2 * HEAD_DIM), axis=2
    )
    key_grad = grouped[:, :, :HEAD_DIM].reshape(own_rows, KV_HEADS * HEAD_DIM).astype(jnp.bfloat16)
    value_grad = (
        grouped[:, :, HEAD_DIM:].reshape(own_rows, KV_HEADS * HEAD_DIM).astype(jnp.bfloat16)
    )
    contract = (((1,), (1,)), ((), ()))
    source_grad = lax.dot_general(
        key_grad, key_weight, contract, preferred_element_type=jnp.float32
    ) + lax.dot_general(value_grad, value_weight, contract, preferred_element_type=jnp.float32)
    picked = query_grad
    normed_grad = summed_on_arrival(
        lax.dot_general(picked, query_weight, contract, preferred_element_type=jnp.float32).astype(
            jnp.bfloat16
        ),
        "tp",
        0,
    )
    scaled_grad = normed_grad * norm_gain
    target_grad = (
        scaled_grad / root_mean
        - target_wide * jnp.mean(scaled_grad * target_wide, axis=1, keepdims=True) / root_mean**3
    )
    picked = normed_all
    query_weight_grad = summed_on_arrival(
        lax.dot_general(
            picked, query_grad, (((0,), (0,)), ((), ())), preferred_element_type=jnp.float32
        ).astype(jnp.bfloat16),
        "sp",
        0,
    )
    return (target_grad, source_grad, query_weight_grad)


def solution(mesh):
    return jax.shard_map(
        shards,
        mesh=mesh,
        in_specs=(
            P(("grp", "sp", "tp"), None),
            P(("grp", "sp", "tp"), None),
            P(),
            P(None, "tp"),
            P(),
            P(),
            P("tp", None),
            P(("grp", "sp"), "tp"),
            P("tp", ("grp", "sp")),
            P(("grp", "sp", "tp"), None),
        ),
        out_specs=(
            P(("grp", "sp", "tp"), None),
            P(("grp", "sp", "tp"), None),
            P(("grp", "sp"), "tp"),
        ),
        check_vma=False,
    )
```

profile of v0, /device:TPU:65, one launch (start us, length us, event | category | flops | bytes accessed | tf_op | source)
XLA Modules:
  0.0 308.8 jit_solution(2163993728256108957)
XLA Ops:
  7.2 0.0 copy-start
  7.2 0.1 all-gather.8.cloned.1.call-start
  7.3 0.9 fusion.43
  8.2 0.8 fusion.45
  9.1 1.4 pad_maximum_fusion.1
  10.4 0.1 all-gather.8.cloned.1.call-update
  10.5 0.1 all-gather.6.cloned.1.call-start
  10.6 0.7 all-gather.6.cloned.1.call-update
  11.3 0.9 copy.20
  12.2 0.7 convert_element_type.126
  12.9 61.8 %all-gather = bf16[1,2048]{1,0:T(2,128)(2,1)S(1)} all-gather(bf16[1,128]{1,0:T(2,128)(2,1)S(1)} %convert_element_type.126), channel_id=2, replica_groups=mesh['grp'=2,'sp'=16,'tp'=16] {'sp'}, dimensions={1}, use_global_device_ids=true | all-gather | bytes 4352 | tf_op jit(solution)/shard_map/all_gather | solution.py:91
  74.7 1.3 constant_dynamic-slice_fusion
  76.0 14.3 %all-gather.8.cloned.1.call-done = bf16[128,4096]{1,0:T(8,128)(2,1)} async-done(((bf16[8,4096]{1,0:T(8,128)(2,1)}), bf16[128,4096]{1,0:T(8,128)(2,1)}) %all-gather.8.cloned.1.call-update) | async-done | bytes 1048592 | tf_op jit(solution)/shard_map/all_gather | solution.py:59
  90.3 1.5 multiply_reduce_fusion
  91.8 23.9 %all-gather.2 = bf16[16,1,128]{2,1,0:T(2,128)(2,1)S(1)} all-gather(bf16[1,1,128]{2,1,0:T(2,128)(2,1)S(1)} %bitcast.104), channel_id=3, replica_groups=mesh['grp'=2,'sp'=16,'tp'=16] {'sp'}, dimensions={0}, use_global_device_ids=true | all-gather | bytes 4352 | tf_op jit(solution)/shard_map/all_gather | solution.py:94
  115.7 0.0 copy-done
  115.7 1.3 convolution_convert_fusion.4
  117.1 25.2 %all_gather.20 = bf16[2048,128]{1,0:T(8,128)(2,1)S(1)} all-gather(bf16[128,128]{1,0:T(8,128)(2,1)S(1)} %convolution_convert_fusion.4), channel_id=1, replica_groups=mesh['grp'=2,'sp'=16,'tp'=16] {'sp'}, dimensions={0}, use_global_device_ids=true | all-gather | bytes 557056 | tf_op jit(solution)/shard_map/all_gather | solution.py:89
  142.3 24.2 %all_gather.22 = bf16[2048,128]{0,1:T(8,128)(2,1)S(1)} all-gather(bf16[128,128]{0,1:T(8,128)(2,1)S(1)} %get-tuple-element.8), channel_id=1, replica_groups=mesh['grp'=2,'sp'=16,'tp'=16] {'sp'}, dimensions={0}, use_global_device_ids=true | all-gather | bytes 557056 | tf_op jit(solution)/shard_map/all_gather | solution.py:90
  166.5 0.0 all-gather.6.cloned.1.call-done
  166.5 3.5 %fusion.17 = bf16[1024,256]{0,1:T(8,128)(2,1)S(1)} fusion(bf16[1024,2048]{1,0:T(8,128)(2,1)} %all-gather.6.cloned.1.call-done, bf16[2048,128]{1,0:T(8,128)(2,1)S(1)} %get-tuple-element.9, bf16[2048,128]{1,0:T(8,128)(2,1)S(1)} %get-tuple-element.10), kind=kOutput, calls=%fused_computation.20 | convolution fusion | flops 1076101120 | bytes 5767168 | tf_op jit(solution)/shard_map/dot_general | solution.py:78
  170.0 1.3 fusion.41
  171.2 0.0 copy-start.1
  171.3 2.9 fusion.2
  174.2 0.0 copy-start.2
  174.2 0.7 fusion.18
  174.9 0.0 copy-done.1
  175.0 0.1 copy.30
  175.1 1.1 copy-done.2
  176.2 0.9 copy.21
  177.1 7.6 %all-to-all-start = ((bf16[16,128,128]{1,2,0:T(8,128)(2,1)}), bf16[16,128,128]{1,2,0:T(8,128)(2,1)S(1)}, u32[]{:S(2)}, u32[]{:S(2)}) async-start(bf16[16,128,128]{1,2,0:T(8,128)(2,1)} %copy.21), calls=%async_computation | async-start | bytes 1048576 | tf_op jit(solution)/shard_map/all_to_all | solution.py:19
  184.6 3.7 %fusion.27 = bf16[1024,1,128]{0,2,1:T(8,128)(2,1)S(1)} fusion(bf16[2048,128]{1,0:T(8,128)(2,1)S(1)} %all_gather.20, bf16[1024,2048,1]{1,0,2:T(8,128)(2,1)} %copy-done.2), kind=kOutput, calls=%fused_computation.24 | convolution fusion | flops 537001984 | bytes 4980736 | tf_op jit(solution)/shard_map/hnm,nhd->md/dot_general | solution.py:105
  188.4 5.3 %fusion.30 = bf16[1024,1,128]{0,2,1:T(8,128)(2,1)S(1)} fusion(bf16[2048,128]{0,1:T(8,128)(2,1)S(1)} %all_gather.22, f32[1024,2048]{1,0:T(8,128)} %copy-done.1, f32[2048]{0:T(1024)S(1)} %bitcast.102), kind=kOutput, calls=%fused_computation.25 | convolution fusion | flops 545390592 | bytes 9183232 | tf_op jit(solution)/shard_map/hnm,nhd->md/dot_general | solution.py:106
  193.7 0.0 copy-start.3
  193.7 0.5 broadcast.79
  194.3 0.0 copy-start.5
  194.3 0.0 copy-start.6
  194.3 1.0 reduce.4
  195.3 0.2 copy.39
  195.5 0.9 reshape.147
  196.4 4.8 %all-to-all-done = bf16[16,128,128]{1,2,0:T(8,128)(2,1)S(1)} async-done(((bf16[16,128,128]{1,2,0:T(8,128)(2,1)}), bf16[16,128,128]{1,2,0:T(8,128)(2,1)S(1)}, u32[]{:S(2)}, u32[]{:S(2)}) %all-to-all-start) | async-done | bytes 524320 | tf_op jit(solution)/shard_map/all_to_all | solution.py:19
  201.2 25.6 %all-to-all-start.2 = ((bf16[16,2,8192]{2,1,0:T(2,128)(2,1)}), bf16[16,2,8192]{2,1,0:T(2,128)(2,1)S(1)}, u32[]{:S(2)}, u32[]{:S(2)}) async-start(bf16[16,2,8192]{2,1,0:T(2,128)(2,1)} %reshape.147), calls=%async_computation.2 | async-start | bytes 1048576 | tf_op jit(solution)/shard_map/all_to_all | solution.py:115
  226.8 0.1 reduce_sum.68
  226.9 1.1 fusion.16
  228.0 16.0 %all-to-all-done.2 = bf16[16,2,8192]{2,1,0:T(2,128)(2,1)S(1)} async-done(((bf16[16,2,8192]{2,1,0:T(2,128)(2,1)}), bf16[16,2,8192]{2,1,0:T(2,128)(2,1)S(1)}, u32[]{:S(2)}, u32[]{:S(2)}) %all-to-all-start.2) | async-done | bytes 524320 | tf_op jit(solution)/shard_map/all_to_all | solution.py:115
  244.0 3.7 %all-to-all-start.1 = ((bf16[16,8,2048]{2,1,0:T(8,128)(2,1)}), bf16[16,8,2048]{2,1,0:T(8,128)(2,1)S(1)}, u32[]{:S(2)}, u32[]{:S(2)}) async-start(bf16[16,8,2048]{2,1,0:T(8,128)(2,1)} %fusion.16), calls=%async_computation.1 | async-start | bytes 1048576 | tf_op jit(solution)/shard_map/all_to_all | solution.py:19
  247.8 2.2 convolution_convert_fusion
  249.9 14.3 %all-to-all-done.1 = bf16[16,8,2048]{2,1,0:T(8,128)(2,1)S(1)} async-done(((bf16[16,8,2048]{2,1,0:T(8,128)(2,1)}), bf16[16,8,2048]{2,1,0:T(8,128)(2,1)S(1)}, u32[]{:S(2)}, u32[]{:S(2)}) %all-to-all-start.1) | async-done | bytes 524320 | tf_op jit(solution)/shard_map/all_to_all | solution.py:19
  264.2 0.0 copy-start.4
  264.2 0.8 copy-done.4
  265.0 6.9 %all-to-all-start.3 = ((bf16[16,128,128]{2,1,0:T(8,128)(2,1)}), bf16[16,128,128]{2,1,0:T(8,128)(2,1)}, u32[]{:S(2)}, u32[]{:S(2)}) async-start(bf16[16,128,128]{2,1,0:T(8,128)(2,1)} %bitcast.18), calls=%async_computation.3 | async-start | bytes 1048576 | tf_op jit(solution)/shard_map/all_to_all | solution.py:19
  271.9 0.5 reshape.148
  272.5 0.1 copy.26
  272.6 0.1 reduce.3
  272.7 0.0 copy-done.3
  272.7 0.4 fusion.51
  273.1 2.5 convolution_add_fusion
  275.6 1.1 convert_reduce_fusion.1
  276.7 0.0 copy-done.5
  276.7 0.0 copy-done.6
  276.7 0.1 fusion.46
  276.9 0.7 fusion.48
  277.6 22.7 %all-to-all-done.3 = bf16[16,128,128]{2,1,0:T(8,128)(2,1)} async-done(((bf16[16,128,128]{2,1,0:T(8,128)(2,1)}), bf16[16,128,128]{2,1,0:T(8,128)(2,1)}, u32[]{:S(2)}, u32[]{:S(2)}) %all-to-all-start.3) | async-done | bytes 524320 | tf_op jit(solution)/shard_map/all_to_all | solution.py:19
  300.2 1.7 convert_reduce_fusion
  (6 shorter events, 0.1 us)
Async XLA Ops:
  7.2 108.5 %copy-start = (bf16[2048,128]{1,0:T(8,128)(2,1)S(1)}, bf16[2048,128]{1,0:T(8,128)(2,1)}, u32[]{:S(2)}) copy-start(bf16[2048,128]{1,0:T(8,128)(2,1)} %param.13) | copy-start | bytes 1572868
  7.2 83.1 %all-gather.8.cloned.1.call-start = ((), (), s32[]{:S(2)}) async-start(), calls=%async_computation.5 | async-start | bytes 1114112 | tf_op jit(solution)/shard_map/all_gather | solution.py:59
  10.5 156.0 %all-gather.6.cloned.1.call-start = ((), (), s32[]{:S(2)}) async-start(), calls=%async_computation.4 | async-start | bytes 4456448 | tf_op jit(solution)/shard_map/all_gather | solution.py:79
  171.2 3.7 %copy-start.1 = (f32[1024,2048]{1,0:T(8,128)}, f32[1024,2048]{1,0:T(8,128)S(1)}, u32[]{:S(2)}) copy-start(f32[1024,2048]{1,0:T(8,128)S(1)} %fusion.41) | copy-start | bytes 25165828
  174.2 2.0 copy-start.2
  177.1 24.1 %all-to-all-start = ((bf16[16,128,128]{1,2,0:T(8,128)(2,1)}), bf16[16,128,128]{1,2,0:T(8,128)(2,1)S(1)}, u32[]{:S(2)}, u32[]{:S(2)}) async-start(bf16[16,128,128]{1,2,0:T(8,128)(2,1)} %copy.21), calls=%async_computation | async-start | bytes 1048576 | tf_op jit(solution)/shard_map/all_to_all | solution.py:19
  193.7 79.0 %copy-start.3 = (bf16[2048,256]{1,0:T(8,128)(2,1)S(1)}, bf16[2048,256]{1,0:T(8,128)(2,1)}, u32[]{:S(2)}) copy-start(bf16[2048,256]{1,0:T(8,128)(2,1)} %param.14) | copy-start | bytes 3145732
  194.3 82.5 %copy-start.5 = (bf16[8,2048]{1,0:T(8,128)(2,1)S(1)}, bf16[8,2048]{1,0:T(8,128)(2,1)}, u32[]{:S(2)}) copy-start(bf16[8,2048]{1,0:T(8,128)(2,1)} %param.10) | copy-start | bytes 98308
  194.3 82.5 %copy-start.6 = (f32[2048]{0:T(1024)S(1)}, f32[2048]{0:T(1024)}, u32[]{:S(2)}) copy-start(f32[2048]{0:T(1024)} %param.12) | copy-start | bytes 24580
  201.2 42.8 %all-to-all-start.2 = ((bf16[16,2,8192]{2,1,0:T(2,128)(2,1)}), bf16[16,2,8192]{2,1,0:T(2,128)(2,1)S(1)}, u32[]{:S(2)}, u32[]{:S(2)}) async-start(bf16[16,2,8192]{2,1,0:T(2,128)(2,1)} %reshape.147), calls=%async_computation.2 | async-start | bytes 1048576 | tf_op jit(solution)/shard_map/all_to_all | solution.py:115
  244.0 20.2 %all-to-all-start.1 = ((bf16[16,8,2048]{2,1,0:T(8,128)(2,1)}), bf16[16,8,2048]{2,1,0:T(8,128)(2,1)S(1)}, u32[]{:S(2)}, u32[]{:S(2)}) async-start(bf16[16,8,2048]{2,1,0:T(8,128)(2,1)} %fusion.16), calls=%async_computation.1 | async-start | bytes 1048576 | tf_op jit(solution)/shard_map/all_to_all | solution.py:19
  264.2 0.8 copy-start.4
  265.0 35.2 %all-to-all-start.3 = ((bf16[16,128,128]{2,1,0:T(8,128)(2,1)}), bf16[16,128,128]{2,1,0:T(8,128)(2,1)}, u32[]{:S(2)}, u32[]{:S(2)}) async-start(bf16[16,128,128]{2,1,0:T(8,128)(2,1)} %bitcast.18), calls=%async_computation.3 | async-start | bytes 1048576 | tf_op jit(solution)/shard_map/all_to_all | solution.py:19
Sparse Core Ops, SparseCore 0:
  10.7 79.5 all-gather.7
  92.4 47.3 all-gather.5
where the time goes:
time: 310 us; the launch traced here: 309 us
  blocking collectives  135 us (44%)
  waiting for transfers between devices  72.8 us (23%)
  starting transfers between devices  43.9 us (14%)
  matrix products  26.5 us (9%)
  between operations  14.3 us (5%)
  other arithmetic  8.82 us (3%)
  local copies, waits for them, and re-layouts  7.37 us (2%)
    all_gather x1, blocking collectives, shards(): lax.all_gather(shift_cols.astype(jnp.bfloat16), 'sp', axis=0, tiled=True)  61.8 us
    all_to_all x3, waiting for transfers between devices, summed_on_arrival(): lax.all_to_all(blocks, axis, split_axis=0, concat_axis=0, tiled=True)  41.7 us
    all_to_all x1, starting transfers between devices, shards(): lax.all_to_all(stacked.astype(jnp.bfloat16), 'tp', split_axis=0, concat_a...  25.6 us
    all_gather x1, blocking collectives, shards(): lax.all_gather(queries, 'sp', axis=0, tiled=True)  25.2 us
    all_gather x1, blocking collectives, shards(): lax.all_gather(out_back, 'sp', axis=0, tiled=True)  24.2 us
    all_gather x1, blocking collectives, shards(): lax.all_gather(drop_cols.astype(jnp.bfloat16), 'sp', axis=0, tiled=True)  23.9 us
    all_to_all x3, starting transfers between devices, summed_on_arrival(): lax.all_to_all(blocks, axis, split_axis=0, concat_axis=0, tiled=True)  18.2 us
    all_to_all x1, waiting for transfers between devices, shards(): lax.all_to_all(stacked.astype(jnp.bfloat16), 'tp', split_axis=0, concat_a...  16 us
  transfers between devices with their start and end apart: 6, of which 5 were waited for; matrix products, arithmetic and copies ran while one was open for 9% of the time, Pallas kernels for 0%

commit v1 on v0

--- a/solution.py
+++ b/solution.py
@@ -6,6 +6,13 @@
 HEADS = 16
 HEAD_DIM = 128
 KV_HEADS = 2
+
+
+def swapped_in(x, axis, d):
+    size = lax.axis_size(axis)
+    blocks = jnp.stack([x for _ in range(size)])
+    blocks = lax.all_to_all(blocks, axis, split_axis=0, concat_axis=0)
+    return jnp.concatenate(blocks, axis=d)
 
 
 def cut_along(array, dim, count):
@@ -86,7 +93,7 @@
     drop_cols = jnp.sum(products.reshape(tgt_local, local_heads, HEAD_DIM), axis=2)
     shift_cols = log_shift.T
     portion = (
-        lax.all_gather(queries, "sp", axis=0, tiled=True),
+        swapped_in(queries, "sp", 0),
         lax.all_gather(out_back, "sp", axis=0, tiled=True),
         lax.all_gather(shift_cols.astype(jnp.bfloat16), "sp", axis=0, tiled=True).astype(
             jnp.float32

time: 310 us -> 342 us (1.10)
  waiting for transfers between devices: 72.8 us -> 137 us
  blocking collectives: 135 us -> 85.9 us
  starting transfers between devices: 43.9 us -> 59.1 us
    all_gather x1, waiting for transfers between devices: 14.3 us -> 78.9 us  [shards(): portion = lax.all_gather(joined, 'tp', axis=0, tiled=True)]
    all_gather x1 -> x0, blocking collectives: 25.2 us -> none  [shards(): lax.all_gather(queries, 'sp', axis=0, tiled=True)]
    all_gather x1, blocking collectives: 61.8 us -> 41.3 us  [shards(): lax.all_gather(shift_cols.astype(jnp.bfloat16), 'sp', axis=0, tiled=True)]
    all_to_all x0 -> x1, starting transfers between devices: none -> 12.8 us  [swapped_in(): blocks = lax.all_to_all(blocks, axis, split_axis=0, concat_axis=0)]
    all_gather x1, blocking collectives: 23.9 us -> 20.4 us  [shards(): lax.all_gather(drop_cols.astype(jnp.bfloat16), 'sp', axis=0, tiled=True)]
  transfers between devices with their start and end apart: 6 -> 7, of which waited for: 5 -> 5; matrix products, arithmetic and copies ran while one was open for 9% -> 9% of each run, Pallas kernels for 0% -> 0%
where the time goes in v1:
time: 342 us; the launch traced here: 340 us
  waiting for transfers between devices  137 us (40%)
  blocking collectives  85.9 us (25%)
  starting transfers between devices  59.1 us (17%)
  matrix products  26.5 us (8%)
  between operations  14.3 us (4%)
  other arithmetic  8.82 us (3%)
  local copies, waits for them, and re-layouts  8.24 us (2%)
    all_gather x1, waiting for transfers between devices, shards(): portion = lax.all_gather(joined, 'tp', axis=0, tiled=True)  78.9 us
    all_to_all x3, waiting for transfers between devices, summed_on_arrival(): lax.all_to_all(blocks, axis, split_axis=0, concat_axis=0, tiled=True)  41.7 us
    all_gather x1, blocking collectives, shards(): lax.all_gather(shift_cols.astype(jnp.bfloat16), 'sp', axis=0, tiled=True)  41.3 us
    all_to_all x1, starting transfers between devices, shards(): lax.all_to_all(stacked.astype(jnp.bfloat16), 'tp', split_axis=0, concat_a...  26.6 us
    all_gather x1, blocking collectives, shards(): lax.all_gather(out_back, 'sp', axis=0, tiled=True)  24.2 us
    all_gather x1, blocking collectives, shards(): lax.all_gather(drop_cols.astype(jnp.bfloat16), 'sp', axis=0, tiled=True)  20.4 us
    all_to_all x3, starting transfers between devices, summed_on_arrival(): lax.all_to_all(blocks, axis, split_axis=0, concat_axis=0, tiled=True)  19.6 us
    all_to_all x1, waiting for transfers between devices, shards(): lax.all_to_all(stacked.astype(jnp.bfloat16), 'tp', split_axis=0, concat_a...  16 us
  transfers between devices with their start and end apart: 7, of which 5 were waited for; matrix products, arithmetic and copies ran while one was open for 9% of the time, Pallas kernels for 0%

profile of v1, /device:TPU:65, one launch (start us, length us, event | category | flops | bytes accessed | tf_op | source)
XLA Modules:
  0.0 340.3 jit_solution(14935696180453917850)
XLA Ops:
  7.2 0.0 copy-start
  7.2 0.1 all-gather.8.cloned.1.call-start
  7.3 0.9 fusion.43
  8.2 0.8 fusion.45
  9.1 1.4 pad_maximum_fusion.1
  10.4 0.1 all-gather.8.cloned.1.call-update
  10.5 0.1 all-gather.6.cloned.1.call-start
  10.6 0.7 all-gather.6.cloned.1.call-update
  11.3 78.9 %all-gather.8.cloned.1.call-done = bf16[128,4096]{1,0:T(8,128)(2,1)} async-done(((bf16[8,4096]{1,0:T(8,128)(2,1)}), bf16[128,4096]{1,0:T(8,128)(2,1)}) %all-gather.8.cloned.1.call-update) | async-done | bytes 1048592 | tf_op jit(solution)/shard_map/all_gather | solution.py:66
  90.2 0.0 copy-done
  90.2 1.3 convolution_convert_fusion.4
  91.6 0.9 stack.2
  92.5 12.8 %all-to-all-start = ((bf16[16,128,128]{2,1,0:T(8,128)(2,1)}), bf16[16,128,128]{2,1,0:T(8,128)(2,1)S(1)}, u32[]{:S(2)}, u32[]{:S(2)}) async-start(bf16[16,128,128]{2,1,0:T(8,128)(2,1)} %stack.2), calls=%async_computation | async-start | bytes 1048576 | tf_op jit(solution)/shard_map/all_to_all | solution.py:14
  105.3 0.9 copy.20
  106.2 0.7 convert_element_type.126
  106.8 41.3 %all-gather = bf16[1,2048]{1,0:T(2,128)(2,1)S(1)} all-gather(bf16[1,128]{1,0:T(2,128)(2,1)S(1)} %convert_element_type.126), channel_id=2, replica_groups=mesh['grp'=2,'sp'=16,'tp'=16] {'sp'}, dimensions={1}, use_global_device_ids=true | all-gather | bytes 4352 | tf_op jit(solution)/shard_map/all_gather | solution.py:98
  148.2 1.3 constant_dynamic-slice_fusion
  149.5 1.5 multiply_reduce_fusion
  151.0 20.4 %all-gather.2 = bf16[16,1,128]{2,1,0:T(2,128)(2,1)S(1)} all-gather(bf16[1,1,128]{2,1,0:T(2,128)(2,1)S(1)} %bitcast.107), channel_id=3, replica_groups=mesh['grp'=2,'sp'=16,'tp'=16] {'sp'}, dimensions={0}, use_global_device_ids=true | all-gather | bytes 4352 | tf_op jit(solution)/shard_map/all_gather | solution.py:101
  171.3 24.2 %all_gather.18 = bf16[2048,128]{0,1:T(8,128)(2,1)S(1)} all-gather(bf16[128,128]{0,1:T(8,128)(2,1)S(1)} %get-tuple-element.8), channel_id=1, replica_groups=mesh['grp'=2,'sp'=16,'tp'=16] {'sp'}, dimensions={0}, use_global_device_ids=true | all-gather | bytes 557056 | tf_op jit(solution)/shard_map/all_gather | solution.py:97
  195.6 0.0 all-gather.6.cloned.1.call-done
  195.6 3.5 %fusion.17 = bf16[1024,256]{0,1:T(8,128)(2,1)S(1)} fusion(bf16[1024,2048]{1,0:T(8,128)(2,1)} %all-gather.6.cloned.1.call-done, bf16[2048,128]{1,0:T(8,128)(2,1)S(1)} %get-tuple-element.9, bf16[2048,128]{1,0:T(8,128)(2,1)S(1)} %get-tuple-element.10), kind=kOutput, calls=%fused_computation.20 | convolution fusion | flops 1076101120 | bytes 5767168 | tf_op jit(solution)/shard_map/dot_general | solution.py:85
  199.1 0.0 all-to-all-done
  199.1 1.3 fusion.41
  200.4 0.0 copy-start.1
  200.4 2.9 fusion.2
  203.3 0.0 copy-start.2
  203.3 0.7 fusion.18
  204.0 0.0 copy-done.1
  204.1 0.1 copy.30
  204.2 1.1 copy-done.2
  205.2 0.9 copy.21
  206.2 9.0 %all-to-all-start.1 = ((bf16[16,128,128]{1,2,0:T(8,128)(2,1)}), bf16[16,128,128]{1,2,0:T(8,128)(2,1)S(1)}, u32[]{:S(2)}, u32[]{:S(2)}) async-start(bf16[16,128,128]{1,2,0:T(8,128)(2,1)} %copy.21), calls=%async_computation.1 | async-start | bytes 1048576 | tf_op jit(solution)/shard_map/all_to_all | solution.py:26
  215.1 3.7 %fusion.27 = bf16[1024,1,128]{0,2,1:T(8,128)(2,1)S(1)} fusion(bf16[2048,128]{1,0:T(8,128)(2,1)S(1)} %bitcast.101, bf16[1024,2048,1]{1,0,2:T(8,128)(2,1)} %copy-done.2), kind=kOutput, calls=%fused_computation.24 | convolution fusion | flops 537001984 | bytes 4980736 | tf_op jit(solution)/shard_map/hnm,nhd->md/dot_general | solution.py:112
  218.8 5.3 %fusion.30 = bf16[1024,1,128]{0,2,1:T(8,128)(2,1)S(1)} fusion(bf16[2048,128]{0,1:T(8,128)(2,1)S(1)} %all_gather.18, f32[1024,2048]{1,0:T(8,128)} %copy-done.1, f32[2048]{0:T(1024)S(1)} %bitcast.105), kind=kOutput, calls=%fused_computation.25 | convolution fusion | flops 545390592 | bytes 9183232 | tf_op jit(solution)/shard_map/hnm,nhd->md/dot_general | solution.py:113
  224.2 0.0 copy-start.3
  224.2 0.5 broadcast.81
  224.7 0.0 copy-start.6
  224.7 1.0 reduce.4
  225.8 0.2 copy.39
  226.0 0.9 reshape.151
  226.9 4.8 %all-to-all-done.1 = bf16[16,128,128]{1,2,0:T(8,128)(2,1)S(1)} async-done(((bf16[16,128,128]{1,2,0:T(8,128)(2,1)}), bf16[16,128,128]{1,2,0:T(8,128)(2,1)S(1)}, u32[]{:S(2)}, u32[]{:S(2)}) %all-to-all-start.1) | async-done | bytes 524320 | tf_op jit(solution)/shard_map/all_to_all | solution.py:26
  231.7 26.6 %all-to-all-start.3 = ((bf16[16,2,8192]{2,1,0:T(2,128)(2,1)}), bf16[16,2,8192]{2,1,0:T(2,128)(2,1)S(1)}, u32[]{:S(2)}, u32[]{:S(2)}) async-start(bf16[16,2,8192]{2,1,0:T(2,128)(2,1)} %reshape.151), calls=%async_computation.3 | async-start | bytes 1048576 | tf_op jit(solution)/shard_map/all_to_all | solution.py:122
  258.3 0.1 reduce_sum.68
  258.3 1.1 fusion.16
  259.5 16.0 %all-to-all-done.3 = bf16[16,2,8192]{2,1,0:T(2,128)(2,1)S(1)} async-done(((bf16[16,2,8192]{2,1,0:T(2,128)(2,1)}), bf16[16,2,8192]{2,1,0:T(2,128)(2,1)S(1)}, u32[]{:S(2)}, u32[]{:S(2)}) %all-to-all-start.3) | async-done | bytes 524320 | tf_op jit(solution)/shard_map/all_to_all | solution.py:122
  275.5 3.7 %all-to-all-start.2 = ((bf16[16,8,2048]{2,1,0:T(8,128)(2,1)}), bf16[16,8,2048]{2,1,0:T(8,128)(2,1)S(1)}, u32[]{:S(2)}, u32[]{:S(2)}) async-start(bf16[16,8,2048]{2,1,0:T(8,128)(2,1)} %fusion.16), calls=%async_computation.2 | async-start | bytes 1048576 | tf_op jit(solution)/shard_map/all_to_all | solution.py:26
  279.2 2.2 convolution_convert_fusion
  281.4 14.3 %all-to-all-done.2 = bf16[16,8,2048]{2,1,0:T(8,128)(2,1)S(1)} async-done(((bf16[16,8,2048]{2,1,0:T(8,128)(2,1)}), bf16[16,8,2048]{2,1,0:T(8,128)(2,1)S(1)}, u32[]{:S(2)}, u32[]{:S(2)}) %all-to-all-start.2) | async-done | bytes 524320 | tf_op jit(solution)/shard_map/all_to_all | solution.py:26
  295.7 0.8 copy-done.4
  296.5 6.9 %all-to-all-start.4 = ((bf16[16,128,128]{2,1,0:T(8,128)(2,1)}), bf16[16,128,128]{2,1,0:T(8,128)(2,1)}, u32[]{:S(2)}, u32[]{:S(2)}) async-start(bf16[16,128,128]{2,1,0:T(8,128)(2,1)} %bitcast.19), calls=%async_computation.4 | async-start | bytes 1048576 | tf_op jit(solution)/shard_map/all_to_all | solution.py:26
  303.4 0.5 reshape.152
  303.9 0.1 copy.26
  304.0 0.1 reduce.3
  304.1 0.0 copy-done.3
  304.1 0.4 fusion.51
  304.6 2.5 convolution_add_fusion
  307.0 1.1 convert_reduce_fusion.1
  308.2 0.0 copy-done.5
  308.2 0.0 copy-done.6
  308.2 0.1 fusion.46
  308.3 0.7 fusion.48
  309.0 22.7 %all-to-all-done.4 = bf16[16,128,128]{2,1,0:T(8,128)(2,1)} async-done(((bf16[16,128,128]{2,1,0:T(8,128)(2,1)}), bf16[16,128,128]{2,1,0:T(8,128)(2,1)}, u32[]{:S(2)}, u32[]{:S(2)}) %all-to-all-start.4) | async-done | bytes 524320 | tf_op jit(solution)/shard_map/all_to_all | solution.py:26
  331.7 1.7 convert_reduce_fusion
  (8 shorter events, 0.1 us)
Async XLA Ops:
  7.2 83.1 %copy-start = (bf16[2048,128]{1,0:T(8,128)(2,1)S(1)}, bf16[2048,128]{1,0:T(8,128)(2,1)}, u32[]{:S(2)}) copy-start(bf16[2048,128]{1,0:T(8,128)(2,1)} %param.13) | copy-start | bytes 1572868
  7.2 83.0 %all-gather.8.cloned.1.call-start = ((), (), s32[]{:S(2)}) async-start(), calls=%async_computation.6 | async-start | bytes 1114112 | tf_op jit(solution)/shard_map/all_gather | solution.py:66
  10.5 185.1 %all-gather.6.cloned.1.call-start = ((), (), s32[]{:S(2)}) async-start(), calls=%async_computation.5 | async-start | bytes 4456448 | tf_op jit(solution)/shard_map/all_gather | solution.py:86
  92.5 106.6 %all-to-all-start = ((bf16[16,128,128]{2,1,0:T(8,128)(2,1)}), bf16[16,128,128]{2,1,0:T(8,128)(2,1)S(1)}, u32[]{:S(2)}, u32[]{:S(2)}) async-start(bf16[16,128,128]{2,1,0:T(8,128)(2,1)} %stack.2), calls=%async_computation | async-start | bytes 1048576 | tf_op jit(solution)/shard_map/all_to_all | solution.py:14
  200.4 3.7 %copy-start.1 = (f32[1024,2048]{1,0:T(8,128)}, f32[1024,2048]{1,0:T(8,128)S(1)}, u32[]{:S(2)}) copy-start(f32[1024,2048]{1,0:T(8,128)S(1)} %fusion.41) | copy-start | bytes 25165828
  203.3 1.9 copy-start.2
  206.2 25.5 %all-to-all-start.1 = ((bf16[16,128,128]{1,2,0:T(8,128)(2,1)}), bf16[16,128,128]{1,2,0:T(8,128)(2,1)S(1)}, u32[]{:S(2)}, u32[]{:S(2)}) async-start(bf16[16,128,128]{1,2,0:T(8,128)(2,1)} %copy.21), calls=%async_computation.1 | async-start | bytes 1048576 | tf_op jit(solution)/shard_map/all_to_all | solution.py:26
  224.2 80.0 %copy-start.3 = (bf16[2048,256]{1,0:T(8,128)(2,1)S(1)}, bf16[2048,256]{1,0:T(8,128)(2,1)}, u32[]{:S(2)}) copy-start(bf16[2048,256]{1,0:T(8,128)(2,1)} %param.14) | copy-start | bytes 3145732
  224.7 83.4 %copy-start.5 = (bf16[8,2048]{1,0:T(8,128)(2,1)S(1)}, bf16[8,2048]{1,0:T(8,128)(2,1)}, u32[]{:S(2)}) copy-start(bf16[8,2048]{1,0:T(8,128)(2,1)} %param.10) | copy-start | bytes 98308
  224.7 83.4 %copy-start.6 = (f32[2048]{0:T(1024)S(1)}, f32[2048]{0:T(1024)}, u32[]{:S(2)}) copy-start(f32[2048]{0:T(1024)} %param.12) | copy-start | bytes 24580
  231.7 43.8 %all-to-all-start.3 = ((bf16[16,2,8192]{2,1,0:T(2,128)(2,1)}), bf16[16,2,8192]{2,1,0:T(2,128)(2,1)S(1)}, u32[]{:S(2)}, u32[]{:S(2)}) async-start(bf16[16,2,8192]{2,1,0:T(2,128)(2,1)} %reshape.151), calls=%async_computation.3 | async-start | bytes 1048576 | tf_op jit(solution)/shard_map/all_to_all | solution.py:122
  275.5 20.2 %all-to-all-start.2 = ((bf16[16,8,2048]{2,1,0:T(8,128)(2,1)}), bf16[16,8,2048]{2,1,0:T(8,128)(2,1)S(1)}, u32[]{:S(2)}, u32[]{:S(2)}) async-start(bf16[16,8,2048]{2,1,0:T(8,128)(2,1)} %fusion.16), calls=%async_computation.2 | async-start | bytes 1048576 | tf_op jit(solution)/shard_map/all_to_all | solution.py:26
  295.7 0.8 copy-start.4
  296.5 35.2 %all-to-all-start.4 = ((bf16[16,128,128]{2,1,0:T(8,128)(2,1)}), bf16[16,128,128]{2,1,0:T(8,128)(2,1)}, u32[]{:S(2)}, u32[]{:S(2)}) async-start(bf16[16,128,128]{2,1,0:T(8,128)(2,1)} %bitcast.19), calls=%async_computation.4 | async-start | bytes 1048576 | tf_op jit(solution)/shard_map/all_to_all | solution.py:26
Sparse Core Ops, SparseCore 0:
  10.7 79.4 all-gather.7
  92.4 47.4 all-gather.5
